TPU v7x, 32 devices: a whole 2x2x4 slice. The times are simulated.
32 devices in a mesh: ep: 8 (over z, x), tp: 4 (over y, core).
Axes of the slice: x: 2, y: 2, z: 4, core: 2. Of those that a mesh axis runs over, the one named last changes fastest.
Arguments:
- tokens: bfloat16 [192, 4096], P('ep'), may hold values from -6 to 6
- norm_gain: bfloat16 [4096], replicated, may hold values from 0.099609375 to 1.8984375
- w_query: bfloat16 [4096, 1024], P('ep', 'tp'), may hold values from -0.09375 to 0.09375
- w_key: bfloat16 [4096, 1024], P('ep', 'tp'), may hold values from -0.09375 to 0.09375
- w_value: bfloat16 [4096, 2048], P('ep', 'tp'), may hold values from -0.09375 to 0.09375
- w_rgate: bfloat16 [4096, 2048], P('ep', 'tp'), may hold values from -0.09375 to 0.09375
- w_decay: bfloat16 [4096, 1024], P('ep', 'tp'), may hold values from -0.375 to 0.375
- decay_shift: float32 [192, 1024], P('ep', 'tp'), may hold values from -2 to 0
- state: float32 [192, 8, 128, 256], P('ep', 'tp'), may hold values from -6 to 6
- head_gain: bfloat16 [2048], P('tp'), may hold values from 0.099609375 to 1.8984375
- w_out: bfloat16 [2048, 4096], P('tp', 'ep'), may hold values from -0.125 to 0.125
- ffn_gain: bfloat16 [4096], replicated, may hold values from 0.099609375 to 1.8984375
- w_gate: bfloat16 [8, 4096, 1024], P('ep', None, 'tp'), may hold values from -0.21875 to 0.21875
- w_lin: bfloat16 [8, 4096, 1024], P('ep', None, 'tp'), may hold values from -0.21875 to 0.21875
- w_down: bfloat16 [8, 1024, 4096], P('ep', 'tp'), may hold values from -0.046875 to 0.046875
- expert_ids: int32 [192, 4], P('ep'), may hold values from 0 to 7, all different within a row; in each aligned block of 24 rows (0 to 23, 24 to 47, ...) at most 24 rows name the same one
- route_weight: float32 [192, 4], P('ep'), may hold values from 0.2 to 1
Outputs:
- result: bfloat16 [192, 4096], P('ep')
Inputs may be any that keep to these rules, and one draw needn't show every extreme that they name: `expert_ids`: each row names 4 different experts; among the rows of one index of ep no expert is named more than 24 times, a bound that some block reaches.
All inputs are finite; a program needn't handle non-finite values.
Results may differ from a plain program's by a relative error of at most 0.022.
Values may be sent and summed in bfloat16 or wider, within the bound.
A program may use at most 128 MiB of HBM per device.

v0:
```python
import jax
import jax.numpy as jnp
from jax import lax
from jax.sharding import PartitionSpec as P

eps = 1e-06
tau = 16.0
limit = 7.0
glu_alpha = 1.702


def rms_scale(values, gain):
    meansq = jnp.mean(values * values, axis=-1, keepdims=True)
    return values * lax.rsqrt(meansq + eps) * gain


def activate(gate, linear):
    gate = jnp.minimum(gate, limit)
    linear = jnp.clip(linear, -limit, limit)
    return (gate * jax.nn.sigmoid(glu_alpha * gate) * (linear + 1.0)).astype(jnp.bfloat16)


def on_device(
    tokens,
    norm_gain,
    w_query,
    w_key,
    w_value,
    w_rgate,
    w_decay,
    decay_shift,
    state,
    head_gain,
    w_out,
    ffn_gain,
    w_gate,
    w_lin,
    w_down,
    expert_ids,
    route_weight,
):
    seq_dev = tokens.shape[0]
    width = tokens.shape[1]
    heads_dev = state.shape[1]
    key_dim = state.shape[2]
    val_dim = state.shape[3]
    key_cols = w_query.shape[1]
    val_cols = w_value.shape[1]
    inputs = tokens.astype(jnp.float32)
    normed = rms_scale(inputs, norm_gain.astype(jnp.float32)).astype(jnp.bfloat16)
    spread = lax.all_to_all(normed, "ep", split_axis=1, concat_axis=0, tiled=True)
    joined = jnp.concatenate((w_query, w_key, w_decay, w_value, w_rgate), axis=1)
    projected = lax.psum_scatter(
        jnp.dot(spread, joined, preferred_element_type=jnp.float32),
        "ep",
        scatter_dimension=0,
        tiled=True,
    )
    projected = projected.astype(jnp.bfloat16).astype(jnp.float32)
    q_rows = projected[:, :key_cols].reshape(seq_dev, heads_dev, key_dim) * key_dim ** (-0.5)
    k_rows = projected[:, key_cols : 2 * key_cols].reshape(seq_dev, heads_dev, key_dim)
    decay_pre = projected[:, 2 * key_cols : 3 * key_cols]
    v_rows = projected[:, 3 * key_cols : 3 * key_cols + val_cols].reshape(
        seq_dev, heads_dev, val_dim
    )
    rgates = projected[:, 3 * key_cols + val_cols :].reshape(seq_dev, heads_dev, val_dim)
    log_decay = jax.nn.log_sigmoid(decay_pre) / tau + decay_shift
    new_state = (
        jnp.exp(log_decay.reshape(seq_dev, heads_dev, key_dim))[..., None] * state
        + k_rows[..., None] * v_rows[:, :, None, :]
    )
    read = jnp.einsum("shk,shkv->shv", q_rows, new_state, precision=lax.Precision.HIGHEST)
    gated = rms_scale(
        read, head_gain.astype(jnp.float32).reshape(heads_dev, val_dim)
    ) * jax.nn.silu(rgates)
    gated = gated.reshape(seq_dev, heads_dev * val_dim).astype(jnp.bfloat16)
    partial_value = jnp.dot(
        lax.all_gather(gated, "ep", axis=0, tiled=True), w_out, preferred_element_type=jnp.float32
    )
    summed = lax.psum(partial_value.astype(jnp.bfloat16), "tp")
    mixed = lax.all_to_all(summed, "ep", split_axis=0, concat_axis=1, tiled=True)
    stream = inputs + mixed.astype(jnp.float32)
    ffn_in = rms_scale(stream, ffn_gain.astype(jnp.float32)).astype(jnp.bfloat16)
    n_ep = lax.axis_size("ep")
    exp_dev = w_gate.shape[0]
    experts = exp_dev * n_ep
    top = expert_ids.shape[1]
    capacity = max(2, 2 * seq_dev * top // experts)
    flat_ids = expert_ids.reshape(-1)
    onehot = (flat_ids[:, None] == jnp.arange(experts, dtype=jnp.int32)[None, :]).astype(jnp.int32)
    rank = jnp.sum((jnp.cumsum(onehot, axis=0) - onehot) * onehot, axis=1)
    slot_of = flat_ids * capacity + rank
    dispatch = (
        jnp.arange(experts * capacity, dtype=jnp.int32)[:, None] == slot_of[None, :]
    ).astype(jnp.bfloat16)
    dispatch = jnp.sum(dispatch.reshape(experts * capacity, seq_dev, top), axis=2)
    outbound = jnp.dot(dispatch, ffn_in, preferred_element_type=jnp.float32).astype(jnp.bfloat16)
    outbound = outbound.reshape(experts, capacity, width)
    arrived = lax.all_to_all(outbound, "ep", split_axis=0, concat_axis=0, tiled=True)
    count = arrived.shape[1]
    rows = arrived.reshape(n_ep, exp_dev, count, width)
    gate = jnp.einsum("secd,edh->sech", rows, w_gate, preferred_element_type=jnp.float32)
    linear = jnp.einsum("secd,edh->sech", rows, w_lin, preferred_element_type=jnp.float32)
    act = activate(gate, linear)
    partial_out = jnp.einsum("sech,ehd->secd", act, w_down, preferred_element_type=jnp.float32)
    summed_out = lax.psum(partial_out.astype(jnp.bfloat16), "tp")
    returned = lax.all_to_all(
        summed_out.reshape(n_ep * exp_dev, count, width),
        "ep",
        split_axis=0,
        concat_axis=0,
        tiled=True,
    )
    picked = (
        returned.reshape(experts * capacity, width)[slot_of]
        .astype(jnp.float32)
        .reshape(seq_dev, top, width)
    )
    routed = jnp.sum(picked * route_weight[..., None], axis=1)
    return (stream + routed).astype(jnp.bfloat16)


def solution(mesh):
    placed = (
        P("ep", None),
        P(),
        P("ep", "tp"),
        P("ep", "tp"),
        P("ep", "tp"),
        P("ep", "tp"),
        P("ep", "tp"),
        P("ep", "tp"),
        P("ep", "tp", None, None),
        P("tp"),
        P("tp", "ep"),
        P(),
        P("ep", None, "tp"),
        P("ep", None, "tp"),
        P("ep", "tp", None),
        P("ep", None),
        P("ep", None),
    )
    return jax.shard_map(
        on_device, mesh=mesh, in_specs=placed, out_specs=P("ep", None), check_vma=False
    )
```

profile of v0, /device:TPU:0, one launch (start us, length us, event | category | flops | bytes accessed | tf_op | source)
XLA Modules:
  0.0 322.8 jit_solution(11763685602241706706)
XLA Ops:
  6.5 0.9 convert_element_type.78
  7.4 1.1 fusion.38
  8.5 1.1 fusion.40
  9.6 0.7 copy.50
  10.3 7.3 %all-to-all-start = ((bf16[24,8,512]{2,0,1:T(8,128)(2,1)}), bf16[24,8,512]{2,0,1:T(8,128)(2,1)S(1)}, u32[]{:S(2)}, u32[]{:S(2)}) async-start(bf16[24,8,512]{2,0,1:T(8,128)(2,1)} %bitcast.95), calls=%async_computation | async-start | bytes 393216 | tf_op jit(solution)/shard_map/all_to_all | solution.py:51
  17.6 1.7 constant_dynamic-update-slice_fusion.4
  19.3 1.7 constant_dynamic-update-slice_fusion.3
  21.0 1.7 constant_dynamic-update-slice_fusion.2
  22.7 0.9 constant_dynamic-update-slice_fusion.1
  23.6 0.9 constant_dynamic-update-slice_fusion
  24.5 1.0 all-to-all-done
  25.5 3.2 fusion.72
  29.0 65.7 %reduce-scatter.2.cloned.1.call-done = f32[24,1792]{1,0:T(8,128)} async-done(((f32[192,1792]{1,0:T(8,128)}), f32[24,1792]{1,0:T(8,128)}) %reduce-scatter.2.cloned.1.call-update) | async-done | bytes 172048 | tf_op jit(solution)/shard_map/reduce_scatter | solution.py:53
  94.7 0.9 convert_convert_fusion
  95.8 6.1 %fusion = f32[24,2,1,256]{3,2,1,0:T(1,128)S(1)} fusion(f32[24,2,128,1]{2,3,1,0:T(1,128)S(1)} %bitcast.103, f32[24,2,128,256]{3,2,1,0:T(8,128)} %param.25, f32[24,2,256]{2,1,0:T(2,128)S(1)} %mul.158, f32[24,2,128]{2,1,0:T(2,128)S(1)} %mul.156, f32[24,2,128]{2,1,0:T(2,128)S(1)} %exp.24), kind=kOutput, calls=%fused_computation.1 | convolution fusion | flops 23592960 | bytes 6463488 | tf_op jit(solution)/shard_map/shk,shkv->shv/dot_general | solution.py:72
  102.2 30.6 %all_gather.3 = bf16[192,512]{1,0:T(8,128)(2,1)S(1)} all-gather(bf16[24,512]{1,0:T(8,128)(2,1)S(1)} %bitcast.104), channel_id=1, replica_groups=mesh['ep'=8,'tp'=4] {'ep'}, dimensions={0}, use_global_device_ids=true | all-gather | bytes 221184 | tf_op jit(solution)/shard_map/all_gather | solution.py:78
  132.9 1.0 convolution_convert_fusion.2
  134.1 30.6 %all-reduce.3.cloned.1.call-done = bf16[8,24,512]{2,1,0:T(8,128)(2,1)} async-done(((bf16[8,24,512]{2,1,0:T(8,128)(2,1)}), bf16[8,24,512]{2,1,0:T(8,128)(2,1)}) %all-reduce.3.cloned.1.call-update) | async-done | bytes 196624 | tf_op jit(solution)/shard_map/psum | solution.py:80
  164.6 5.5 %all-to-all-start.1 = ((bf16[8,24,512]{2,1,0:T(8,128)(2,1)}), bf16[8,24,512]{2,1,0:T(8,128)(2,1)S(1)}, u32[]{:S(2)}, u32[]{:S(2)}) async-start(bf16[8,24,512]{2,1,0:T(8,128)(2,1)} %all-reduce.3.cloned.1.call-done), calls=%async_computation.2 | async-start | bytes 393216 | tf_op jit(solution)/shard_map/all_to_all | solution.py:81
  170.7 7.3 %all-to-all-done.1 = bf16[8,24,512]{2,1,0:T(8,128)(2,1)S(1)} async-done(((bf16[8,24,512]{2,1,0:T(8,128)(2,1)}), bf16[8,24,512]{2,1,0:T(8,128)(2,1)S(1)}, u32[]{:S(2)}, u32[]{:S(2)}) %all-to-all-start.1) | async-done | bytes 196640 | tf_op jit(solution)/shard_map/all_to_all | solution.py:81
  178.2 0.6 convolution_convert_fusion.1
  178.9 37.3 %all_to_all.42 = bf16[8,24,4096]{2,1,0:T(8,128)(2,1)S(1)} all-to-all(bf16[8,24,4096]{2,1,0:T(8,128)(2,1)S(1)} %bitcast.96), channel_id=1, replica_groups=mesh['ep'=8,'tp'=4] {'ep'}, dimensions={0} | all-to-all | bytes 3145728 | tf_op jit(solution)/shard_map/all_to_all | solution.py:99
  216.2 1.2 copy-done.1
  217.4 0.6 fusion.27
  218.0 5.1 %convolution_convert_fusion = bf16[8,24,4096]{2,1,0:T(8,128)(2,1)} fusion(bf16[1,256,4096]{2,1,0:T(8,128)(2,1)S(1)} %copy-done, bf16[8,24,4096]{2,1,0:T(8,128)(2,1)} %copy-done.1, bf16[1,4096,256]{2,1,0:T(8,128)(2,1)} %param.30, f32[8,1,24,256]{3,2,0,1:T(8,128)S(1)} %fusion.27), kind=kOutput, calls=%fused_computation.5 | convolution fusion | flops 806535168 | bytes 7536640 | tf_op jit(solution)/shard_map/sech,ehd->secd/dot_general | solution.py:105
  223.1 42.3 %all-reduce.5.cloned.1.call-done = bf16[8,24,4096]{2,1,0:T(8,128)(2,1)} async-done(((bf16[8,24,4096]{2,1,0:T(8,128)(2,1)}), bf16[8,24,4096]{2,1,0:T(8,128)(2,1)}) %all-reduce.5.cloned.1.call-update) | async-done | bytes 1572880 | tf_op jit(solution)/shard_map/psum | solution.py:106
  265.5 5.5 %all-to-all-start.3 = ((bf16[8,24,4096]{2,1,0:T(8,128)(2,1)}), bf16[8,24,4096]{2,1,0:T(8,128)(2,1)}, u32[]{:S(2)}, u32[]{:S(2)}) async-start(bf16[8,24,4096]{2,1,0:T(8,128)(2,1)} %all-reduce.5.cloned.1.call-done), calls=%async_computation.4 | async-start | bytes 3145728 | tf_op jit(solution)/shard_map/all_to_all | solution.py:107
  271.2 36.8 %all-to-all-done.3 = bf16[8,24,4096]{2,1,0:T(8,128)(2,1)} async-done(((bf16[8,24,4096]{2,1,0:T(8,128)(2,1)}), bf16[8,24,4096]{2,1,0:T(8,128)(2,1)}, u32[]{:S(2)}, u32[]{:S(2)}) %all-to-all-start.3) | async-done | bytes 1572896 | tf_op jit(solution)/shard_map/all_to_all | solution.py:107
  308.0 3.4 %gather_fusion = bf16[96,4096]{1,0:T(8,128)(2,1)S(1)} fusion(bf16[192,4096]{1,0:T(8,128)(2,1)} %bitcast.22, s32[1024]{0:T(1024)S(1)} %pad_clamp_fusion), kind=kCustom, calls=%fused_computation | custom fusion | bytes 1573248 | tf_op jit(solution)/shard_map/gather | solution.py:115
  311.4 1.6 reshape.151
  313.0 2.5 multiply_reduce_fusion
  315.5 0.7 add_convert_fusion
  (60 shorter events, 1.9 us)
Async XLA Ops:
  6.5 211.5 %copy-start = (bf16[1,256,4096]{2,1,0:T(8,128)(2,1)S(1)}, bf16[1,256,4096]{2,1,0:T(8,128)(2,1)}, u32[]{:S(2)}) copy-start(bf16[1,256,4096]{2,1,0:T(8,128)(2,1)} %param.31) | copy-start | bytes 6291460
  6.5 16.1 %copy-start.5 = (bf16[512,512]{1,0:T(8,128)(2,1)S(1)}, bf16[512,512]{1,0:T(8,128)(2,1)}, u32[]{:S(2)}) copy-start(bf16[512,512]{1,0:T(8,128)(2,1)} %param.21) | copy-start | bytes 1572868
  8.5 15.1 %copy-start.6 = (bf16[512,512]{1,0:T(8,128)(2,1)S(1)}, bf16[512,512]{1,0:T(8,128)(2,1)}, u32[]{:S(2)}) copy-start(bf16[512,512]{1,0:T(8,128)(2,1)} %param.22) | copy-start | bytes 1572868
  10.3 15.2 %all-to-all-start = ((bf16[24,8,512]{2,0,1:T(8,128)(2,1)}), bf16[24,8,512]{2,0,1:T(8,128)(2,1)S(1)}, u32[]{:S(2)}, u32[]{:S(2)}) async-start(bf16[24,8,512]{2,0,1:T(8,128)(2,1)} %bitcast.95), calls=%async_computation | async-start | bytes 393216 | tf_op jit(solution)/shard_map/all_to_all | solution.py:51
  17.6 77.2 %reduce-scatter.2.cloned.1.call-start = ((), (), s32[]{:S(2)}) async-start(), calls=%async_computation.5 | async-start | bytes 1548288 | tf_op jit(solution)/shard_map/reduce_scatter | solution.py:53
  25.5 3.2 %copy-start.11 = (bf16[512]{0:T(512)(128)(2,1)S(1)}, bf16[512]{0:T(512)(128)(2,1)}, u32[]{:S(2)}) copy-start(bf16[512]{0:T(512)(128)(2,1)} %param.26) | copy-start | bytes 3076
  25.5 3.3 %copy-start.9 = (s32[24,4]{0,1:T(4,128)S(1)}, s32[24,4]{0,1:T(4,128)}, u32[]{:S(2)}) copy-start(s32[24,4]{0,1:T(4,128)} %param.32) | copy-start | bytes 1156
  25.5 70.2 %copy-start.7 = (f32[24,256]{1,0:T(8,128)S(1)}, f32[24,256]{1,0:T(8,128)}, u32[]{:S(2)}) copy-start(f32[24,256]{1,0:T(8,128)} %param.24) | copy-start | bytes 73732
  28.7 135.9 %all-reduce.3.cloned.1.call-start = ((), (), s32[]{:S(2)}) async-start(), calls=%async_computation.6 | async-start | bytes 393216 | tf_op jit(solution)/shard_map/psum | solution.py:80
  95.8 37.0 %copy-start.4 = (bf16[512,512]{1,0:T(8,128)(2,1)S(1)}, bf16[512,512]{1,0:T(8,128)(2,1)}, u32[]{:S(2)}) copy-start(bf16[512,512]{1,0:T(8,128)(2,1)} %param.27) | copy-start | bytes 1572868
  101.9 68.7 %copy-start.8 = (bf16[4096]{0:T(1024)(128)(2,1)S(1)}, bf16[4096]{0:T(1024)(128)(2,1)}, u32[]{:S(2)}) copy-start(bf16[4096]{0:T(1024)(128)(2,1)} %param.28) | copy-start | bytes 24580
  102.1 76.0 %copy-start.2 = (bf16[24,4096]{1,0:T(8,128)(2,1)S(1)}, bf16[24,4096]{1,0:T(8,128)(2,1)}, u32[]{:S(2)}) copy-start(bf16[24,4096]{1,0:T(8,128)(2,1)} %param.17) | copy-start | bytes 589828
  164.6 13.3 %all-to-all-start.1 = ((bf16[8,24,512]{2,1,0:T(8,128)(2,1)}), bf16[8,24,512]{2,1,0:T(8,128)(2,1)S(1)}, u32[]{:S(2)}, u32[]{:S(2)}) async-start(bf16[8,24,512]{2,1,0:T(8,128)(2,1)} %all-reduce.3.cloned.1.call-done), calls=%async_computation.2 | async-start | bytes 393216 | tf_op jit(solution)/shard_map/all_to_all | solution.py:81
  170.2 95.3 %all-reduce.5.cloned.1.call-start = ((), (), s32[]{:S(2)}) async-start(), calls=%async_computation.7 | async-start | bytes 3145728 | tf_op jit(solution)/shard_map/psum | solution.py:106
  178.8 38.5 %copy-start.3 = (bf16[1,4096,256]{2,1,0:T(8,128)(2,1)S(1)}, bf16[1,4096,256]{2,1,0:T(8,128)(2,1)}, u32[]{:S(2)}) copy-start(bf16[1,4096,256]{2,1,0:T(8,128)(2,1)} %param.29) | copy-start | bytes 6291460
  216.2 1.2 copy-start.1
  223.1 47.9 %copy-start.10 = (f32[24,4]{0,1:T(4,128)S(1)}, f32[24,4]{0,1:T(4,128)}, u32[]{:S(2)}) copy-start(f32[24,4]{0,1:T(4,128)} %param.33) | copy-start | bytes 1156
  265.5 42.5 %all-to-all-start.3 = ((bf16[8,24,4096]{2,1,0:T(8,128)(2,1)}), bf16[8,24,4096]{2,1,0:T(8,128)(2,1)}, u32[]{:S(2)}, u32[]{:S(2)}) async-start(bf16[8,24,4096]{2,1,0:T(8,128)(2,1)} %all-reduce.5.cloned.1.call-done), calls=%async_computation.4 | async-start | bytes 3145728 | tf_op jit(solution)/shard_map/all_to_all | solution.py:107
Sparse Core Ops, SparseCore 0:
  28.8 65.8 reduce-scatter.1
  134.0 30.6 all-reduce.2
  223.2 42.1 all-reduce.4
where the time goes:
time: 323 us
  waiting for transfers between devices  184 us (57%)
  blocking collectives  68 us (21%)
  starting transfers between devices  18.4 us (6%)
  matrix products  16.5 us (5%)
  local copies, waits for them, and re-layouts  14.5 us (4%)
  between operations  13.4 us (4%)
  other arithmetic  8.18 us (3%)
    reduce_scatter x1, waiting for transfers between devices, on_device(): lax.psum_scatter(jnp.dot(spread, joined, preferred_element_type=jnp.float...  65.7 us
    psum x1, waiting for transfers between devices, on_device(): summed_out = lax.psum(partial_out.astype(jnp.bfloat16), 'tp')  42.3 us
    all_to_all x1, blocking collectives, on_device(): lax.all_to_all(outbound, 'ep', split_axis=0, concat_axis=0, tiled=True)  37.3 us
    all_to_all x1, waiting for transfers between devices, on_device(): lax.all_to_all(summed_out.reshape(n_ep * exp_dev, count, width), 'ep', sp...  36.8 us
    all_gather x1, blocking collectives, on_device(): lax.all_gather(gated, 'ep', axis=0, tiled=True)  30.6 us
    psum x1, waiting for transfers between devices, on_device(): summed = lax.psum(partial_value.astype(jnp.bfloat16), 'tp')  30.6 us
    unnamed x31, local copies, waits for them, and re-layouts  7.35 us
    all_to_all x1, starting transfers between devices, on_device(): lax.all_to_all(normed, 'ep', split_axis=1, concat_axis=0, tiled=True)  7.28 us
  transfers between devices with their start and end apart: 6, of which 6 were waited for; matrix products, arithmetic and copies ran while one was open for 2% of the time, Pallas kernels for 0%

commit v1 on v0

--- a/solution.py
+++ b/solution.py
@@ -77,7 +77,7 @@
     partial_value = jnp.dot(
         lax.all_gather(gated, "ep", axis=0, tiled=True), w_out, preferred_element_type=jnp.float32
     )
-    summed = lax.psum(partial_value.astype(jnp.bfloat16), "tp")
+    summed = jnp.sum(lax.all_gather(partial_value.astype(jnp.bfloat16), "tp"), axis=0)
     mixed = lax.all_to_all(summed, "ep", split_axis=0, concat_axis=1, tiled=True)
     stream = inputs + mixed.astype(jnp.float32)
     ffn_in = rms_scale(stream, ffn_gain.astype(jnp.float32)).astype(jnp.bfloat16)

time: 323 us -> 302 us (0.935)
  waiting for transfers between devices: 184 us -> 153 us
  blocking collectives: 68 us -> 79.5 us
    psum x1 -> x0, waiting for transfers between devices: 30.6 us -> none  [on_device(): summed = lax.psum(partial_value.astype(jnp.bfloat16), 'tp')]
    all_gather x0 -> x1, blocking collectives: none -> 8.7 us  [on_device(): lax.all_gather(partial_value.astype(jnp.bfloat16), 'tp')]
  transfers between devices with their start and end apart: 6 -> 5, of which waited for: 6 -> 5; matrix products, arithmetic and copies ran while one was open for 2% -> 3% of each run, Pallas kernels for 0% -> 0%
where the time goes in v1:
time: 302 us
  waiting for transfers between devices  153 us (51%)
  blocking collectives  79.5 us (26%)
  starting transfers between devices  16.3 us (5%)
  matrix products  15.8 us (5%)
  local copies, waits for them, and re-layouts  14.5 us (5%)
  between operations  13.7 us (5%)
  other arithmetic  9 us (3%)
    reduce_scatter x1, waiting for transfers between devices, on_device(): lax.psum_scatter(jnp.dot(spread, joined, preferred_element_type=jnp.float...  65.5 us
    psum x1, waiting for transfers between devices, on_device(): summed_out = lax.psum(partial_out.astype(jnp.bfloat16), 'tp')  41.1 us
    all_to_all x1, blocking collectives, on_device(): lax.all_to_all(outbound, 'ep', split_axis=0, concat_axis=0, tiled=True)  40.2 us
    all_to_all x1, waiting for transfers between devices, on_device(): lax.all_to_all(summed_out.reshape(n_ep * exp_dev, count, width), 'ep', sp...  36.8 us
    all_gather x1, blocking collectives, on_device(): lax.all_gather(gated, 'ep', axis=0, tiled=True)  30.6 us
    all_gather x1, blocking collectives, on_device(): lax.all_gather(partial_value.astype(jnp.bfloat16), 'tp')  8.7 us
    all_to_all x1, waiting for transfers between devices, on_device(): lax.all_to_all(summed, 'ep', split_axis=0, concat_axis=1, tiled=True)  8.16 us
    unnamed x31, local copies, waits for them, and re-layouts  7.37 us
  transfers between devices with their start and end apart: 5, of which 5 were waited for; matrix products, arithmetic and copies ran while one was open for 3% of the time, Pallas kernels for 0%

profile of v1, /device:TPU:0, one launch (start us, length us, event | category | flops | bytes accessed | tf_op | source)
XLA Modules:
  0.0 301.5 jit_solution(16738004663710420703)
XLA Ops:
  6.5 0.9 convert_element_type.80
  7.4 1.1 fusion.38
  8.5 1.1 fusion.40
  9.6 0.7 copy.48
  10.3 7.3 %all-to-all-start = ((bf16[24,8,512]{2,0,1:T(8,128)(2,1)}), bf16[24,8,512]{2,0,1:T(8,128)(2,1)S(1)}, u32[]{:S(2)}, u32[]{:S(2)}) async-start(bf16[24,8,512]{2,0,1:T(8,128)(2,1)} %bitcast.96), calls=%async_computation | async-start | bytes 393216 | tf_op jit(solution)/shard_map/all_to_all | solution.py:51
  17.6 1.7 constant_dynamic-update-slice_fusion.4
  19.3 1.7 constant_dynamic-update-slice_fusion.3
  21.0 1.7 constant_dynamic-update-slice_fusion.2
  22.7 0.9 constant_dynamic-update-slice_fusion.1
  23.6 0.8 constant_dynamic-update-slice_fusion
  24.4 1.1 all-to-all-done
  25.5 3.2 %fusion.72 = f32[192,1792]{1,0:T(8,128)} fusion(bf16[192,512]{1,0:T(8,128)(2,1)S(1)} %bitcast.103, bf16[512,1792]{1,0:T(8,128)(2,1)} %constant_dynamic-update-slice_fusion), kind=kOutput, calls=%fused_computation.89 | convolution fusion | flops 352321536 | bytes 3407872 | tf_op jit(solution)/shard_map/dot_general | solution.py:54
  29.2 65.5 %reduce-scatter.2.cloned.1.call-done = f32[24,1792]{1,0:T(8,128)} async-done(((f32[192,1792]{1,0:T(8,128)}), f32[24,1792]{1,0:T(8,128)}) %reduce-scatter.2.cloned.1.call-update) | async-done | bytes 172048 | tf_op jit(solution)/shard_map/reduce_scatter | solution.py:53
  94.7 0.9 convert_convert_fusion
  95.8 6.1 %fusion = f32[24,2,1,256]{3,2,1,0:T(1,128)S(1)} fusion(f32[24,2,128,1]{2,3,1,0:T(1,128)S(1)} %bitcast.104, f32[24,2,128,256]{3,2,1,0:T(8,128)} %param.25, f32[24,2,256]{2,1,0:T(2,128)S(1)} %mul.158, f32[24,2,128]{2,1,0:T(2,128)S(1)} %mul.156, f32[24,2,128]{2,1,0:T(2,128)S(1)} %exp.24), kind=kOutput, calls=%fused_computation.1 | convolution fusion | flops 23592960 | bytes 6463488 | tf_op jit(solution)/shard_map/shk,shkv->shv/dot_general | solution.py:72
  102.2 30.6 %all_gather.9 = bf16[192,512]{1,0:T(8,128)(2,1)S(1)} all-gather(bf16[24,512]{1,0:T(8,128)(2,1)S(1)} %bitcast.105), channel_id=1, replica_groups=mesh['ep'=8,'tp'=4] {'ep'}, dimensions={0}, use_global_device_ids=true | all-gather | bytes 221184 | tf_op jit(solution)/shard_map/all_gather | solution.py:78
  133.1 8.7 %all-gather = bf16[768,512]{1,0:T(8,128)(2,1)S(1)} all-gather(bf16[192,512]{1,0:T(8,128)(2,1)S(1)} %convolution_convert_fusion.2), channel_id=2, replica_groups=mesh['ep'=8,'tp'=4] {'tp'}, dimensions={0}, use_global_device_ids=true | all-gather | bytes 983040 | tf_op jit(solution)/shard_map/all_gather | solution.py:80
  141.8 0.8 reduce_sum.75
  142.6 3.4 %all-to-all-start.1 = ((bf16[8,24,512]{2,1,0:T(8,128)(2,1)}), bf16[8,24,512]{2,1,0:T(8,128)(2,1)S(1)}, u32[]{:S(2)}, u32[]{:S(2)}) async-start(bf16[8,24,512]{2,1,0:T(8,128)(2,1)} %bitcast.5), calls=%async_computation.2 | async-start | bytes 393216 | tf_op jit(solution)/shard_map/all_to_all | solution.py:81
  146.5 8.2 %all-to-all-done.1 = bf16[8,24,512]{2,1,0:T(8,128)(2,1)S(1)} async-done(((bf16[8,24,512]{2,1,0:T(8,128)(2,1)}), bf16[8,24,512]{2,1,0:T(8,128)(2,1)S(1)}, u32[]{:S(2)}, u32[]{:S(2)}) %all-to-all-start.1) | async-done | bytes 196640 | tf_op jit(solution)/shard_map/all_to_all | solution.py:81
  155.0 0.6 convolution_convert_fusion.1
  155.6 40.2 %all_to_all.42 = bf16[8,24,4096]{2,1,0:T(8,128)(2,1)S(1)} all-to-all(bf16[8,24,4096]{2,1,0:T(8,128)(2,1)S(1)} %bitcast.97), channel_id=1, replica_groups=mesh['ep'=8,'tp'=4] {'ep'}, dimensions={0} | all-to-all | bytes 3145728 | tf_op jit(solution)/shard_map/all_to_all | solution.py:99
  195.8 1.2 copy-done.1
  197.0 0.6 fusion.27
  197.6 5.1 %convolution_convert_fusion = bf16[8,24,4096]{2,1,0:T(8,128)(2,1)} fusion(bf16[1,256,4096]{2,1,0:T(8,128)(2,1)S(1)} %copy-done, bf16[8,24,4096]{2,1,0:T(8,128)(2,1)} %copy-done.1, bf16[1,4096,256]{2,1,0:T(8,128)(2,1)} %param.30, f32[8,1,24,256]{3,2,0,1:T(8,128)S(1)} %fusion.27), kind=kOutput, calls=%fused_computation.5 | convolution fusion | flops 806535168 | bytes 7536640 | tf_op jit(solution)/shard_map/sech,ehd->secd/dot_general | solution.py:105
  202.7 41.1 %all-reduce.2.cloned.1.call-done = bf16[8,24,4096]{2,1,0:T(8,128)(2,1)} async-done(((bf16[8,24,4096]{2,1,0:T(8,128)(2,1)}), bf16[8,24,4096]{2,1,0:T(8,128)(2,1)}) %all-reduce.2.cloned.1.call-update) | async-done | bytes 1572880 | tf_op jit(solution)/shard_map/psum | solution.py:106
  243.9 5.5 %all-to-all-start.3 = ((bf16[8,24,4096]{2,1,0:T(8,128)(2,1)}), bf16[8,24,4096]{2,1,0:T(8,128)(2,1)}, u32[]{:S(2)}, u32[]{:S(2)}) async-start(bf16[8,24,4096]{2,1,0:T(8,128)(2,1)} %all-reduce.2.cloned.1.call-done), calls=%async_computation.4 | async-start | bytes 3145728 | tf_op jit(solution)/shard_map/all_to_all | solution.py:107
  249.6 36.8 %all-to-all-done.3 = bf16[8,24,4096]{2,1,0:T(8,128)(2,1)} async-done(((bf16[8,24,4096]{2,1,0:T(8,128)(2,1)}), bf16[8,24,4096]{2,1,0:T(8,128)(2,1)}, u32[]{:S(2)}, u32[]{:S(2)}) %all-to-all-start.3) | async-done | bytes 1572896 | tf_op jit(solution)/shard_map/all_to_all | solution.py:107
  286.4 3.4 %gather_fusion = bf16[96,4096]{1,0:T(8,128)(2,1)S(1)} fusion(bf16[192,4096]{1,0:T(8,128)(2,1)} %bitcast.23, s32[1024]{0:T(1024)S(1)} %pad_clamp_fusion), kind=kCustom, calls=%fused_computation | custom fusion | bytes 1573248 | tf_op jit(solution)/shard_map/gather | solution.py:115
  289.8 1.6 reshape.151
  291.4 2.5 multiply_reduce_fusion
  293.9 0.7 add_convert_fusion
  (59 shorter events, 2.1 us)
Async XLA Ops:
  6.5 191.0 %copy-start = (bf16[1,256,4096]{2,1,0:T(8,128)(2,1)S(1)}, bf16[1,256,4096]{2,1,0:T(8,128)(2,1)}, u32[]{:S(2)}) copy-start(bf16[1,256,4096]{2,1,0:T(8,128)(2,1)} %param.31) | copy-start | bytes 6291460
  6.5 16.2 %copy-start.5 = (bf16[512,512]{1,0:T(8,128)(2,1)S(1)}, bf16[512,512]{1,0:T(8,128)(2,1)}, u32[]{:S(2)}) copy-start(bf16[512,512]{1,0:T(8,128)(2,1)} %param.21) | copy-start | bytes 1572868
  8.5 15.1 %copy-start.6 = (bf16[512,512]{1,0:T(8,128)(2,1)S(1)}, bf16[512,512]{1,0:T(8,128)(2,1)}, u32[]{:S(2)}) copy-start(bf16[512,512]{1,0:T(8,128)(2,1)} %param.22) | copy-start | bytes 1572868
  10.3 15.2 %all-to-all-start = ((bf16[24,8,512]{2,0,1:T(8,128)(2,1)}), bf16[24,8,512]{2,0,1:T(8,128)(2,1)S(1)}, u32[]{:S(2)}, u32[]{:S(2)}) async-start(bf16[24,8,512]{2,0,1:T(8,128)(2,1)} %bitcast.96), calls=%async_computation | async-start | bytes 393216 | tf_op jit(solution)/shard_map/all_to_all | solution.py:51
  17.6 77.1 %reduce-scatter.2.cloned.1.call-start = ((), (), s32[]{:S(2)}) async-start(), calls=%async_computation.5 | async-start | bytes 1548288 | tf_op jit(solution)/shard_map/reduce_scatter | solution.py:53
  25.5 3.2 %copy-start.11 = (bf16[512]{0:T(512)(128)(2,1)S(1)}, bf16[512]{0:T(512)(128)(2,1)}, u32[]{:S(2)}) copy-start(bf16[512]{0:T(512)(128)(2,1)} %param.26) | copy-start | bytes 3076
  25.5 3.2 %copy-start.9 = (s32[24,4]{0,1:T(4,128)S(1)}, s32[24,4]{0,1:T(4,128)}, u32[]{:S(2)}) copy-start(s32[24,4]{0,1:T(4,128)} %param.32) | copy-start | bytes 1156
  28.7 67.0 %copy-start.7 = (f32[24,256]{1,0:T(8,128)S(1)}, f32[24,256]{1,0:T(8,128)}, u32[]{:S(2)}) copy-start(f32[24,256]{1,0:T(8,128)} %param.24) | copy-start | bytes 73732
  95.8 37.0 %copy-start.4 = (bf16[512,512]{1,0:T(8,128)(2,1)S(1)}, bf16[512,512]{1,0:T(8,128)(2,1)}, u32[]{:S(2)}) copy-start(bf16[512,512]{1,0:T(8,128)(2,1)} %param.27) | copy-start | bytes 1572868
  102.2 44.3 %copy-start.8 = (bf16[4096]{0:T(1024)(128)(2,1)S(1)}, bf16[4096]{0:T(1024)(128)(2,1)}, u32[]{:S(2)}) copy-start(bf16[4096]{0:T(1024)(128)(2,1)} %param.28) | copy-start | bytes 24580
  133.1 21.7 %copy-start.2 = (bf16[24,4096]{1,0:T(8,128)(2,1)S(1)}, bf16[24,4096]{1,0:T(8,128)(2,1)}, u32[]{:S(2)}) copy-start(bf16[24,4096]{1,0:T(8,128)(2,1)} %param.17) | copy-start | bytes 589828
  142.6 12.1 %all-to-all-start.1 = ((bf16[8,24,512]{2,1,0:T(8,128)(2,1)}), bf16[8,24,512]{2,1,0:T(8,128)(2,1)S(1)}, u32[]{:S(2)}, u32[]{:S(2)}) async-start(bf16[8,24,512]{2,1,0:T(8,128)(2,1)} %bitcast.5), calls=%async_computation.2 | async-start | bytes 393216 | tf_op jit(solution)/shard_map/all_to_all | solution.py:81
  146.0 97.8 %all-reduce.2.cloned.1.call-start = ((), (), s32[]{:S(2)}) async-start(), calls=%async_computation.6 | async-start | bytes 3145728 | tf_op jit(solution)/shard_map/psum | solution.py:106
  155.6 41.3 %copy-start.3 = (bf16[1,4096,256]{2,1,0:T(8,128)(2,1)S(1)}, bf16[1,4096,256]{2,1,0:T(8,128)(2,1)}, u32[]{:S(2)}) copy-start(bf16[1,4096,256]{2,1,0:T(8,128)(2,1)} %param.29) | copy-start | bytes 6291460
  195.8 1.2 copy-start.1
  202.7 46.8 %copy-start.10 = (f32[24,4]{0,1:T(4,128)S(1)}, f32[24,4]{0,1:T(4,128)}, u32[]{:S(2)}) copy-start(f32[24,4]{0,1:T(4,128)} %param.33) | copy-start | bytes 1156
  243.9 42.5 %all-to-all-start.3 = ((bf16[8,24,4096]{2,1,0:T(8,128)(2,1)}), bf16[8,24,4096]{2,1,0:T(8,128)(2,1)}, u32[]{:S(2)}, u32[]{:S(2)}) async-start(bf16[8,24,4096]{2,1,0:T(8,128)(2,1)} %all-reduce.2.cloned.1.call-done), calls=%async_computation.4 | async-start | bytes 3145728 | tf_op jit(solution)/shard_map/all_to_all | solution.py:107
Sparse Core Ops, SparseCore 0:
  28.8 65.8 reduce-scatter.1
  202.8 40.9 all-reduce.1
